TPU v7x, 32 devices: a whole 2x2x4 slice. The times are simulated.
32 devices in a mesh: sp: 8 (over z, y), dp: 4 (over x, core).
Axes of the slice: x: 2, y: 2, z: 4, core: 2. Of those that a mesh axis runs over, the one named last changes fastest.
Arguments:
- queries: bfloat16 [4, 1024, 1024], P('dp', 'sp'), may hold values from -6 to 6
- keys: bfloat16 [4, 1024, 256], P('dp', 'sp'), may hold values from -6 to 6
- values: bfloat16 [4, 1024, 256], P('dp', 'sp'), may hold values from -6 to 6
- q_gain: float32 [64], replicated, may hold values from 0.55 to 8
- k_gain: float32 [64], replicated, may hold values from 0.55 to 8
- residual: bfloat16 [4, 1024, 2048], P('dp', 'sp'), may hold values from -6 to 6
- out_weight: bfloat16 [1024, 2048], replicated, may hold values from -0.1875 to 0.1875
- mix_gain: float32 [2048], replicated, may hold values from 0.1 to 1.9
- ffn_gain: float32 [2048], replicated, may hold values from 0.1 to 1.9
- post_gain: float32 [2048], replicated, may hold values from 0.1 to 1.9
- expert_ids: int32 [4, 1024, 2], P('dp', 'sp'), may hold values from 0 to 31, all different within a row; in each aligned block of 128 rows (0 to 127, 128 to 255, ..., all dimensions but the last counted through in order) at most 16 rows name the same one
- expert_gate: float32 [4, 1024, 2], P('dp', 'sp'), may hold values from 0.05 to 1
- w_gate: bfloat16 [32, 2048, 512], P(('sp', 'dp')), may hold values from -0.125 to 0.125
- w_up: bfloat16 [32, 2048, 512], P(('sp', 'dp')), may hold values from -0.125 to 0.125
- w_down: bfloat16 [32, 512, 2048], P(('sp', 'dp')), may hold values from -0.25 to 0.25
Outputs:
- result: bfloat16 [4, 1024, 2048], P('dp', 'sp')
Inputs may be any that keep to these rules, and one draw needn't show every extreme that they name: `expert_ids`: each token names 2 different experts; among the 128 tokens of one device no expert is named more than 16 times, and that bound is reached.
All inputs are finite; a program needn't handle non-finite values.
Results may differ from a plain program's by a relative error of at most 0.0085.
The roundings to bfloat16 on the way count: a program that leaves them out, or rounds other values in their place, can miss the bound.
Values may be sent and summed in bfloat16 or wider, within the bound.
A program may use at most 64 MiB of HBM per device.

v0:
```python
import jax
import jax.numpy as jnp
from jax import lax
from jax.sharding import PartitionSpec as P

D = 2048
GRID = 64


eps_norm = 1e-06
theta_base = 10000.0
block_rows = 512


def rms_scale(values):
    return values * lax.rsqrt(jnp.mean(values * values, axis=-1, keepdims=True) + eps_norm)


def rotate(field, gain):
    seq_len, head_count, head_size = field.shape
    values = rms_scale(field.astype(jnp.float32)) * gain
    positions = jnp.arange(seq_len, dtype=jnp.int32)
    row_index = (positions // GRID).astype(jnp.float32)
    col_index = (positions % GRID).astype(jnp.float32)
    pair_quarter = head_size // 4
    frequency = theta_base ** (-(4.0 * jnp.arange(pair_quarter, dtype=jnp.float32)) / head_size)
    angles = jnp.concatenate(
        [row_index[:, None] * frequency, col_index[:, None] * frequency], axis=1
    )
    cosine_table = jnp.cos(angles)[:, None, :]
    sine_table = jnp.sin(angles)[:, None, :]
    paired = values.reshape(seq_len, head_count, head_size // 2, 2)
    even_part = paired[..., 0]
    odd_part = paired[..., 1]
    turned = jnp.stack(
        [
            even_part * cosine_table - odd_part * sine_table,
            even_part * sine_table + odd_part * cosine_table,
        ],
        axis=-1,
    )
    return turned.reshape(seq_len, head_count, head_size).astype(jnp.bfloat16)


def attend(q_turned, k_turned, v_rows):
    seq_len, q_count, head_size = q_turned.shape
    kv_count = k_turned.shape[1]
    group_size = q_count // kv_count

    def one_block(start):
        q_block = lax.dynamic_slice_in_dim(q_turned, start, block_rows, 0)
        q_block = q_block.reshape(block_rows, kv_count, group_size, head_size)
        scores = jnp.einsum(
            "qkgd,skd->kgqs", q_block, k_turned, preferred_element_type=jnp.float32
        ) * head_size ** (-0.5)
        row_max = jnp.max(scores, axis=-1, keepdims=True)
        exp_scores = jnp.exp(scores - row_max)
        weights = (exp_scores / jnp.sum(exp_scores, axis=-1, keepdims=True)).astype(jnp.bfloat16)
        summed = jnp.einsum("kgqs,skd->qkgd", weights, v_rows, preferred_element_type=jnp.float32)
        return summed.astype(jnp.bfloat16).reshape(block_rows, q_count * head_size)

    starts = jnp.arange(seq_len // block_rows, dtype=jnp.int32) * block_rows
    return lax.map(one_block, starts).reshape(seq_len, q_count * head_size)


def shards(
    queries,
    keys,
    values,
    q_gain,
    k_gain,
    residual,
    out_weight,
    mix_gain,
    ffn_gain,
    post_gain,
    expert_ids,
    expert_gate,
    w_gate,
    w_up,
    w_down,
):
    sp_count = lax.axis_size("sp")
    dp_count = lax.axis_size("dp")
    tok_rows = queries.shape[1]
    head_size = q_gain.shape[0]
    heads_q = queries.shape[2] // head_size
    heads_kv = keys.shape[2] // head_size
    q_here = heads_q // sp_count
    kv_here = max(q_here * heads_kv // heads_q, 1)
    copies = kv_here * sp_count // heads_kv
    key_rows = jnp.repeat(keys[0].reshape(tok_rows, heads_kv, head_size), copies, axis=1).reshape(
        tok_rows, -1
    )
    value_rows = jnp.repeat(
        values[0].reshape(tok_rows, heads_kv, head_size), copies, axis=1
    ).reshape(tok_rows, -1)
    q_heads, k_heads, v_heads = (
        lax.all_to_all(queries[0], "sp", split_axis=1, concat_axis=0, tiled=True),
        lax.all_to_all(key_rows, "sp", split_axis=1, concat_axis=0, tiled=True),
        lax.all_to_all(value_rows, "sp", split_axis=1, concat_axis=0, tiled=True),
    )
    seq_len = q_heads.shape[0]
    q_turned = rotate(q_heads.reshape(seq_len, q_here, head_size), q_gain)
    k_turned = rotate(k_heads.reshape(seq_len, kv_here, head_size), k_gain)
    attended = attend(q_turned, k_turned, v_heads.reshape(seq_len, kv_here, head_size))
    token_side = lax.all_to_all(attended, "sp", split_axis=0, concat_axis=1, tiled=True)
    projected = jnp.dot(token_side, out_weight, preferred_element_type=jnp.float32)
    first_res = (residual[0].astype(jnp.float32) + rms_scale(projected) * mix_gain).astype(
        jnp.bfloat16
    )
    normed = (rms_scale(first_res.astype(jnp.float32)) * ffn_gain).astype(jnp.bfloat16)
    experts_all = sp_count * dp_count
    top_n = expert_ids.shape[2]
    capacity = 2 * tok_rows * top_n // experts_all
    flat_ids = expert_ids[0].reshape(-1)
    onehot = (flat_ids[:, None] == jnp.arange(experts_all, dtype=jnp.int32)[None, :]).astype(
        jnp.int32
    )
    running = jnp.cumsum(onehot, axis=0) - onehot
    slot_index = jnp.sum(running * onehot, axis=1)
    target = flat_ids * capacity + slot_index
    sources = jnp.repeat(normed, top_n, axis=0)
    outbox = jnp.zeros((experts_all * capacity, D), jnp.bfloat16).at[target].set(sources)
    outbox = outbox.reshape(experts_all, capacity, D)
    arrived = lax.all_to_all(outbox, ("sp", "dp"), split_axis=0, concat_axis=0, tiled=True)
    layout = arrived.shape
    flattened = arrived.reshape(-1, layout[-1])
    gate_value = jnp.dot(flattened, w_gate[0], preferred_element_type=jnp.float32)
    up_value = jnp.dot(flattened, w_up[0], preferred_element_type=jnp.float32)
    hidden = (jax.nn.silu(gate_value) * up_value).astype(jnp.bfloat16)
    answer = jnp.dot(hidden, w_down[0], preferred_element_type=jnp.float32).astype(jnp.bfloat16)
    returned = lax.all_to_all(
        answer.reshape(layout), ("sp", "dp"), split_axis=0, concat_axis=0, tiled=True
    )
    flat_back = returned.reshape(experts_all * capacity, D)
    answers = flat_back[target].astype(jnp.float32).reshape(tok_rows, top_n, D)
    expert_sum = jnp.sum(answers * expert_gate[0][:, :, None], axis=1)
    result = (first_res.astype(jnp.float32) + rms_scale(expert_sum) * post_gain).astype(
        jnp.bfloat16
    )
    return result[None]


def solution(mesh):
    return jax.shard_map(
        shards,
        mesh=mesh,
        in_specs=(
            P("dp", "sp", None),
            P("dp", "sp", None),
            P("dp", "sp", None),
            P(),
            P(),
            P("dp", "sp", None),
            P(),
            P(),
            P(),
            P(),
            P("dp", "sp", None),
            P("dp", "sp", None),
            P(("sp", "dp"), None, None),
            P(("sp", "dp"), None, None),
            P(("sp", "dp"), None, None),
        ),
        out_specs=P("dp", "sp", None),
        check_vma=False,
    )
```

profile of v0, /device:TPU:0, one launch (start us, length us, event | category | flops | bytes accessed | tf_op | source)
XLA Modules:
  0.0 212.4 jit_solution(9765671484295745760)
XLA Ops:
  1.8 7.3 %all-to-all-start.1 = ((bf16[128,8,64]{0,2,1:T(8,128)(2,1)}), bf16[128,8,64]{0,2,1:T(8,128)(2,1)S(1)}, u32[]{:S(2)}, u32[]{:S(2)}) async-start(bf16[128,8,64]{0,2,1:T(8,128)(2,1)} %bitcast.20), calls=%async_computation.1 | async-start | bytes 262144 | tf_op jit(solution)/shard_map/all_to_all | solution.py:100
  10.7 1.8 copy.77
  16.6 1.2 fusion.42
  18.4 6.0 %all-to-all-start.2 = ((bf16[128,8,64]{0,2,1:T(8,128)(2,1)}), bf16[128,8,64]{0,2,1:T(8,128)(2,1)S(1)}, u32[]{:S(2)}, u32[]{:S(2)}) async-start(bf16[128,8,64]{0,2,1:T(8,128)(2,1)} %bitcast.27), calls=%async_computation.2 | async-start | bytes 262144 | tf_op jit(solution)/shard_map/all_to_all | solution.py:101
  24.8 6.9 %all-to-all-done.2 = bf16[128,8,64]{0,2,1:T(8,128)(2,1)S(1)} async-done(((bf16[128,8,64]{0,2,1:T(8,128)(2,1)}), bf16[128,8,64]{0,2,1:T(8,128)(2,1)S(1)}, u32[]{:S(2)}, u32[]{:S(2)}) %all-to-all-start.2) | async-done | bytes 131104 | tf_op jit(solution)/shard_map/all_to_all | solution.py:101
  31.8 3.4 %all-to-all-start = ((bf16[128,8,128]{0,2,1:T(8,128)(2,1)}), bf16[128,8,128]{0,2,1:T(8,128)(2,1)S(1)}, u32[]{:S(2)}, u32[]{:S(2)}) async-start(bf16[128,8,128]{0,2,1:T(8,128)(2,1)} %bitcast.16), calls=%async_computation | async-start | bytes 524288 | tf_op jit(solution)/shard_map/all_to_all | solution.py:99
  36.8 6.5 %all-to-all-done = bf16[128,8,128]{0,2,1:T(8,128)(2,1)S(1)} async-done(((bf16[128,8,128]{0,2,1:T(8,128)(2,1)}), bf16[128,8,128]{0,2,1:T(8,128)(2,1)S(1)}, u32[]{:S(2)}, u32[]{:S(2)}) %all-to-all-start) | async-done | bytes 262176 | tf_op jit(solution)/shard_map/all_to_all | solution.py:99
  47.6 12.1 %while.10 = (s32[]{:T(128)}, bf16[2,512,128]{2,1,0:T(8,128)(2,1)}, s32[2]{0:T(128)S(1)}, bf16[1024,2,64]{0,2,1:T(8,128)(2,1)S(1)}, bf16[1024,1,64]{0,2,1:T(8,128...) while((s32[]{:T(128)}, bf16[2,512,128]{2,1,0:T(8,128)(2,1)}, ...), condition=%wide.region_5.6_spmd, body=%wide.region_2.5_spmd.sunk | while | flops 277936128 | bytes 13652623 | solution.py:63
  57.8 1.2 fusion.71
  59.7 3.6 %all-to-all-start.3 = ((bf16[8,128,128]{2,1,0:T(8,128)(2,1)}), bf16[8,128,128]{2,1,0:T(8,128)(2,1)S(1)}, u32[]{:S(2)}, u32[]{:S(2)}) async-start(bf16[8,128,128]{2,1,0:T(8,128)(2,1)} %bitcast.29), calls=%async_computation.3 | async-start | bytes 524288 | tf_op jit(solution)/shard_map/all_to_all | solution.py:107
  63.7 7.6 %all-to-all-done.3 = bf16[8,128,128]{2,1,0:T(8,128)(2,1)S(1)} async-done(((bf16[8,128,128]{2,1,0:T(8,128)(2,1)}), bf16[8,128,128]{2,1,0:T(8,128)(2,1)S(1)}, u32[]{:S(2)}, u32[]{:S(2)}) %all-to-all-start.3) | async-done | bytes 262176 | tf_op jit(solution)/shard_map/all_to_all | solution.py:107
  71.5 3.1 %multiply_reduce_fusion.2 = (f32[128]{0:T(128)S(1)}, f32[128,2048]{1,0:T(8,128)S(1)}) fusion(bf16[128,1024]{0,1:T(8,128)(2,1)S(1)} %bitcast.148, bf16[1024,2048]{1,0:T(8,128)(2,1)} %param.23), kind=kOutput, calls=%fused_computation.39 | convolution fusion | flops 537395072 | bytes 5505536 | tf_op jit(solution)/shard_map/dot_general | solution.py:108
  75.5 1.6 broadcast_in_dim.19
  77.1 2.3 %reshape.518 = bf16[256,2048]{1,0:T(8,128)(2,1)} reshape(bf16[128,2,2048]{2,1,0:T(2,128)(2,1)} %broadcast_in_dim.19) | data formatting | bytes 2097152 | tf_op jit(solution)/shard_map/reshape | solution.py:123
  79.3 4.4 %scatter_custom_fusion = bf16[512,2048]{1,0:T(8,128)(2,1)} fusion(s32[256]{0:T(256)S(1)} %bitcast.153, bf16[256,2048]{1,0:T(8,128)(2,1)} %reshape.518, bf16[]{:T(256)} %constant.76.clone.1), kind=kCustom, calls=%fused_computation.37 | custom fusion | bytes 2097664 | tf_op jit(solution)/shard_map/scatter | solution.py:124
  83.8 51.5 %all_to_all.71 = bf16[32,16,2048]{2,1,0:T(8,128)(2,1)S(1)} all-to-all(bf16[32,16,2048]{2,1,0:T(8,128)(2,1)} %bitcast.143), channel_id=1, replica_groups=mesh['sp'=8,'dp'=4] {'sp','dp'}, dimensions={0} | all-to-all | bytes 4194304 | tf_op jit(solution)/shard_map/all_to_all | solution.py:126
  135.3 1.3 copy-done.1
  136.6 2.2 %fusion.17 = f32[512,512]{1,0:T(8,128)} fusion(bf16[512,2048]{1,0:T(8,128)(2,1)S(1)} %bitcast.146, bf16[1,2048,512]{2,1,0:T(8,128)(2,1)S(1)} %copy-done.15), kind=kOutput, calls=%fused_computation.22 | convolution fusion | flops 1073741824 | bytes 5242880 | tf_op jit(solution)/shard_map/dot_general | solution.py:129
  138.8 6.3 %convolution_convert_fusion = bf16[512,2048]{1,0:T(8,128)(2,1)} fusion(bf16[1,512,2048]{2,1,0:T(8,128)(2,1)S(1)} %copy-done, bf16[512,2048]{1,0:T(8,128)(2,1)} %bitcast.147, bf16[1,2048,512]{2,1,0:T(8,128)(2,1)} %param.30, f32[512,512]{1,0:T(8,128)} %fusion.17), kind=kOutput, calls=%fused_computation.18 | convolution fusion | flops 2150105088 | bytes 9437184 | tf_op jit(solution)/shard_map/dot_general | solution.py:132
  145.1 4.0 %all-to-all-start.5 = ((bf16[32,16,2048]{2,1,0:T(8,128)(2,1)}), bf16[32,16,2048]{2,1,0:T(8,128)(2,1)}, u32[]{:S(2)}, u32[]{:S(2)}) async-start(bf16[32,16,2048]{2,1,0:T(8,128)(2,1)} %bitcast.145), calls=%async_computation.5 | async-start | bytes 4194304 | tf_op jit(solution)/shard_map/all_to_all | solution.py:133
  149.3 48.5 %all-to-all-done.5 = bf16[32,16,2048]{2,1,0:T(8,128)(2,1)} async-done(((bf16[32,16,2048]{2,1,0:T(8,128)(2,1)}), bf16[32,16,2048]{2,1,0:T(8,128)(2,1)}, u32[]{:S(2)}, u32[]{:S(2)}) %all-to-all-start.5) | async-done | bytes 2097184 | tf_op jit(solution)/shard_map/all_to_all | solution.py:133
  197.8 5.2 %gather_fusion = bf16[256,2048]{1,0:T(8,128)(2,1)} fusion(bf16[512,2048]{1,0:T(8,128)(2,1)} %bitcast.41, s32[1024]{0:T(1024)S(1)} %pad_clamp_fusion), kind=kCustom, calls=%fused_computation | custom fusion | bytes 2098176 | tf_op jit(solution)/shard_map/gather | solution.py:137
  203.0 3.4 %reshape.505 = f32[128,2,2048]{2,1,0:T(2,128)} reshape(bf16[256,2048]{1,0:T(8,128)(2,1)} %gather_fusion) | data formatting | bytes 3145728 | tf_op jit(solution)/shard_map/convert_element_type | solution.py:137
  206.4 4.8 %multiply_reduce_fusion = f32[128,2048]{1,0:T(8,128)S(1)} fusion(f32[128,2,2048]{2,1,0:T(2,128)} %reshape.505, f32[128,2]{1,0:T(8,128)S(1)} %copy.93), kind=kLoop, calls=%fused_computation.24 | loop fusion | flops 786432 | bytes 3146752 | tf_op jit(solution)/shard_map/reduce_sum | solution.py:138
  (105 shorter events, 24.5 us)
Async XLA Ops:
  0.0 138.8 %copy-start = (bf16[1,512,2048]{2,1,0:T(8,128)(2,1)S(1)}, bf16[1,512,2048]{2,1,0:T(8,128)(2,1)}, u32[]{:S(2)}) copy-start(bf16[1,512,2048]{2,1,0:T(8,128)(2,1)} %param.31) | copy-start | bytes 6291460
  1.8 16.0 %all-to-all-start.1 = ((bf16[128,8,64]{0,2,1:T(8,128)(2,1)}), bf16[128,8,64]{0,2,1:T(8,128)(2,1)S(1)}, u32[]{:S(2)}, u32[]{:S(2)}) async-start(bf16[128,8,64]{0,2,1:T(8,128)(2,1)} %bitcast.20), calls=%async_computation.1 | async-start | bytes 262144 | tf_op jit(solution)/shard_map/all_to_all | solution.py:100
  15.7 8.8 %copy-start.5 = (s32[32,2,128]{2,0,1:T(8,128)}, s32[32,2,128]{2,0,1:T(8,128)S(1)}, u32[]{:S(2)}) copy-start(s32[32,2,128]{2,0,1:T(8,128)S(1)} %reduce-window.6) | copy-start | bytes 98308
  15.9 8.5 %copy-start.11 = (s32[32,3]{0,1:T(4,128)}, s32[32,3]{0,1:T(4,128)S(1)}, u32[]{:S(2)}) copy-start(s32[32,3]{0,1:T(4,128)S(1)} %reduce-window.9) | copy-start | bytes 1156
  18.4 13.3 %all-to-all-start.2 = ((bf16[128,8,64]{0,2,1:T(8,128)(2,1)}), bf16[128,8,64]{0,2,1:T(8,128)(2,1)S(1)}, u32[]{:S(2)}, u32[]{:S(2)}) async-start(bf16[128,8,64]{0,2,1:T(8,128)(2,1)} %bitcast.27), calls=%async_computation.2 | async-start | bytes 262144 | tf_op jit(solution)/shard_map/all_to_all | solution.py:101
  31.8 11.6 %all-to-all-start = ((bf16[128,8,128]{0,2,1:T(8,128)(2,1)}), bf16[128,8,128]{0,2,1:T(8,128)(2,1)S(1)}, u32[]{:S(2)}, u32[]{:S(2)}) async-start(bf16[128,8,128]{0,2,1:T(8,128)(2,1)} %bitcast.16), calls=%async_computation | async-start | bytes 524288 | tf_op jit(solution)/shard_map/all_to_all | solution.py:99
  43.8 2.3 %copy-start.2 = (f32[1024,32]{0,1:T(8,128)S(1)}, f32[1024,32]{0,1:T(8,128)}, u32[]{:S(2)}) copy-start(f32[1024,32]{0,1:T(8,128)} %get-tuple-element.58) | copy-start | bytes 393220
  43.8 2.3 %copy-start.3 = (f32[1024,32]{0,1:T(8,128)S(1)}, f32[1024,32]{0,1:T(8,128)}, u32[]{:S(2)}) copy-start(f32[1024,32]{0,1:T(8,128)} %get-tuple-element.59) | copy-start | bytes 393220
  45.1 2.4 %copy-start.7 = (bf16[1024,1,64]{0,2,1:T(8,128)(2,1)S(1)}, bf16[1024,1,64]{0,2,1:T(8,128)(2,1)}, u32[]{:S(2)}) copy-start(bf16[1024,1,64]{0,2,1:T(8,128)(2,1)} %reshape.495) | copy-start | bytes 393220
  45.1 2.4 %copy-start.16 = (s32[2]{0:T(128)S(1)}, s32[2]{0:T(128)}, u32[]{:S(2)}) copy-start(s32[2]{0:T(128)} %iota_multiply_fusion) | copy-start | bytes 28
  47.6 15.8 %copy-start.13 = (s32[1,128,2]{1,2,0:T(2,128)S(1)}, s32[1,128,2]{1,2,0:T(2,128)}, u32[]{:S(2)}) copy-start(s32[1,128,2]{1,2,0:T(2,128)} %param.27) | copy-start | bytes 3076
  47.6 16.0 %copy-start.6 = (s32[32,2,128]{2,0,1:T(8,128)S(1)}, s32[32,2,128]{2,0,1:T(8,128)}, u32[]{:S(2)}) copy-start(s32[32,2,128]{2,0,1:T(8,128)} %copy-done.5) | copy-start | bytes 98308
  47.6 16.0 %slice-start = ((s32[32,3]{0,1:T(4,128)}), s32[32,2]{0,1:T(2,128)S(1)}, s32[]{:S(2)}) async-start(s32[32,3]{0,1:T(4,128)} %copy-done.11), calls=%async_computation.6 | async-start | bytes 2048 | tf_op jit(solution)/shard_map/slice.1
  47.6 16.0 %copy-start.12 = (s32[256]{0:T(256)S(1)}, s32[256]{0:T(256)}, u32[]{:S(2)}) copy-start(s32[256]{0:T(256)} %eq.28) | copy-start | bytes 3076
  59.7 11.6 %all-to-all-start.3 = ((bf16[8,128,128]{2,1,0:T(8,128)(2,1)}), bf16[8,128,128]{2,1,0:T(8,128)(2,1)S(1)}, u32[]{:S(2)}, u32[]{:S(2)}) async-start(bf16[8,128,128]{2,1,0:T(8,128)(2,1)} %bitcast.29), calls=%async_computation.3 | async-start | bytes 524288 | tf_op jit(solution)/shard_map/all_to_all | solution.py:107
  71.5 3.1 %copy-start.4 = (bf16[1,128,2048]{2,1,0:T(8,128)(2,1)S(1)}, bf16[1,128,2048]{2,1,0:T(8,128)(2,1)}, u32[]{:S(2)}) copy-start(bf16[1,128,2048]{2,1,0:T(8,128)(2,1)} %param.22) | copy-start | bytes 1572868
  71.5 3.1 %copy-start.8 = (f32[2048]{0:T(1024)S(1)}, f32[2048]{0:T(1024)}, u32[]{:S(2)}) copy-start(f32[2048]{0:T(1024)} %param.24) | copy-start | bytes 24580
  74.6 0.7 copy-start.9
  83.8 52.9 %copy-start.15 = (bf16[1,2048,512]{2,1,0:T(8,128)(2,1)S(1)}, bf16[1,2048,512]{2,1,0:T(8,128)(2,1)}, u32[]{:S(2)}) copy-start(bf16[1,2048,512]{2,1,0:T(8,128)(2,1)} %param.29) | copy-start | bytes 6291460
  135.3 1.3 copy-start.1
  145.1 4.0 %copy-start.14 = (f32[1,128,2]{1,2,0:T(2,128)S(1)}, f32[1,128,2]{1,2,0:T(2,128)}, u32[]{:S(2)}) copy-start(f32[1,128,2]{1,2,0:T(2,128)} %param.28) | copy-start | bytes 3076
  145.1 52.7 %all-to-all-start.5 = ((bf16[32,16,2048]{2,1,0:T(8,128)(2,1)}), bf16[32,16,2048]{2,1,0:T(8,128)(2,1)}, u32[]{:S(2)}, u32[]{:S(2)}) async-start(bf16[32,16,2048]{2,1,0:T(8,128)(2,1)} %bitcast.145), calls=%async_computation.5 | async-start | bytes 4194304 | tf_op jit(solution)/shard_map/all_to_all | solution.py:133
  206.3 5.0 %copy-start.10 = (f32[2048]{0:T(1024)S(1)}, f32[2048]{0:T(1024)}, u32[]{:S(2)}) copy-start(f32[2048]{0:T(1024)} %param.26) | copy-start | bytes 24580
where the time goes:
time: 213 us; the launch traced here: 212 us
  waiting for transfers between devices  69.5 us (33%)
  blocking collectives  51.5 us (24%)
  local copies, waits for them, and re-layouts  32.7 us (15%)
  starting transfers between devices  24.3 us (11%)
  matrix products  15.7 us (7%)
  other arithmetic  14.7 us (7%)
  loops' own time  3.4 us (2%)
    all_to_all x1, blocking collectives, shards(): lax.all_to_all(outbox, ('sp', 'dp'), split_axis=0, concat_axis=0, tiled=T...  51.5 us
    all_to_all x1, waiting for transfers between devices, shards(): lax.all_to_all(answer.reshape(layout), ('sp', 'dp'), split_axis=0, concat...  48.5 us
    all_to_all x1, waiting for transfers between devices, shards(): lax.all_to_all(attended, 'sp', split_axis=0, concat_axis=1, tiled=True)  7.57 us
    all_to_all x1, starting transfers between devices, shards(): lax.all_to_all(key_rows, 'sp', split_axis=1, concat_axis=0, tiled=True)  7.31 us
    all_to_all x1, waiting for transfers between devices, shards(): lax.all_to_all(value_rows, 'sp', split_axis=1, concat_axis=0, tiled=True)  6.94 us
    all_to_all x1, waiting for transfers between devices, shards(): lax.all_to_all(queries[0], 'sp', split_axis=1, concat_axis=0, tiled=True)  6.53 us
    unnamed x38, local copies, waits for them, and re-layouts  6.28 us
    dot_general x1, matrix products, shards(): jnp.dot(hidden, w_down[0], preferred_element_type=jnp.float32)  6.26 us
  transfers between devices with their start and end apart: 5, of which 4 were waited for; matrix products, arithmetic and copies ran while one was open for 5% of the time, Pallas kernels for 0%

commit v1 on v0

v1 whole, which is shorter than its diff:
```python
import functools

import jax
import jax.numpy as jnp
import numpy as np
from jax import lax
from jax.experimental import pallas as pl
from jax.experimental.pallas import tpu as pltpu
from jax.sharding import PartitionSpec as P

GRID = 64
LANES = 128
eps_norm = 1e-06
theta_base = 10000.0
MESH = pl.DeviceIdType.MESH
f32 = jnp.float32
bf16 = jnp.bfloat16


def tables(rows, head_size):
    half = head_size // 2
    lane = np.arange(LANES) % head_size
    pair = lane // 2
    quarter = head_size // 4
    by_row = pair < quarter
    frequency = theta_base ** (-(4.0 * (pair % quarter)) / head_size)
    sign = np.where(lane % 2 == 0, -1.0, 1.0)
    a_row = np.arange(rows)[:, None] * frequency
    a_col = np.arange(GRID)[:, None] * frequency
    out = (
        np.where(by_row, np.cos(a_row), 0.0),
        np.where(by_row, np.sin(a_row) * sign, 0.0),
        np.where(by_row, 0.0, np.cos(a_col)),
        np.where(by_row, 0.0, np.sin(a_col) * sign),
    )
    return [jnp.asarray(t, f32) for t in out]


def rms(x):
    return x * lax.rsqrt(jnp.mean(x * x, axis=-1, keepdims=True) + eps_norm)


def dot(a, b):
    return jnp.dot(a, b, preferred_element_type=f32)


def kernel(
    n_sp, n_dp, cap, pitch, groups,
    q_ref, k_ref, v_ref, qg_ref, kg_ref, cr_ref, sr_ref, cc_ref, sc_ref,
    res_ref, mix_ref, ffn_ref, post_ref, ids_ref, gate_ref,
    wo_hbm, wg_hbm, wu_hbm, wd_hbm,
    out_ref,
    kbuf, vbuf, att, first, outbox, arrived, returned, pack, comb_hi, comb_lo,
    wo, wg, wu, wd, w_sem,
    ks_send, ks_recv, vs_send, vs_recv, d_send, d_recv, r_send, r_recv,
):
    n_dev = n_sp * n_dp
    sp = lax.axis_index("sp")
    dp = lax.axis_index("dp")
    tok, q_width = q_ref.shape
    kv_width = k_ref.shape[1]
    head = qg_ref.shape[1]
    d_model = res_ref.shape[1]
    heads_q, heads_kv = q_width // head, kv_width // head
    group = heads_q // heads_kv

    weights = [
        pltpu.make_async_copy(src, dst, w_sem.at[n])
        for n, (src, dst) in enumerate(((wo_hbm, wo), (wg_hbm, wg), (wu_hbm, wu), (wd_hbm, wd)))
    ]
    for w in weights:
        w.start()

    def peer(i):
        return lax.rem(sp + i // n_dp, n_sp), lax.rem(dp + i % n_dp, n_dp)

    def source(i):
        return lax.rem(sp + n_sp - i // n_dp, n_sp), lax.rem(dp + n_dp - i % n_dp, n_dp)

    barrier = pltpu.get_barrier_semaphore()

    def greet(i, c):
        pl.semaphore_signal(barrier, inc=1, device_id=peer(i), device_id_type=MESH)
        return c

    lax.fori_loop(1, n_dev, greet, 0)

    lane = lax.broadcasted_iota(jnp.int32, (tok, LANES), 1)
    even = lane % 2 == 0
    low = lane % (2 * head) < head
    same = (
        lax.broadcasted_iota(jnp.int32, (LANES, LANES), 0) // head
        == lax.broadcasted_iota(jnp.int32, (LANES, LANES), 1) // head
    ).astype(bf16)
    per_dev = tok // GRID
    cos_t = jnp.concatenate(
        [cc_ref[...] + cr_ref[pl.ds(sp * per_dev + u, 1), :] for u in range(per_dev)], axis=0
    )
    sin_t = jnp.concatenate(
        [sc_ref[...] + sr_ref[pl.ds(sp * per_dev + u, 1), :] for u in range(per_dev)], axis=0
    )

    def turn(x, gain):
        x = x.astype(f32)
        square = x * x
        hi = square.astype(bf16)
        lo = (square - hi.astype(f32)).astype(bf16)
        mean = (dot(hi, same) + dot(lo, same)) * (1.0 / head)
        x = x * lax.rsqrt(mean + eps_norm) * gain
        swapped = jnp.where(even, pltpu.roll(x, LANES - 1, 1), pltpu.roll(x, 1, 1))
        return x * cos_t + swapped * sin_t

    k_gain = jnp.concatenate([kg_ref[...]] * (LANES // head), axis=1)
    q_gain = jnp.concatenate([qg_ref[...]] * (LANES // head), axis=1)
    for c in range(kv_width // LANES):
        cols = slice(c * LANES, (c + 1) * LANES)
        kbuf[0, :, cols] = turn(k_ref[:, cols], k_gain).astype(bf16)
    vbuf[0] = v_ref[...]

    pl.semaphore_wait(barrier, n_dev - 1)

    def kv_copies(i):
        to = (lax.rem(sp + i, n_sp), dp)
        return (
            pltpu.make_async_remote_copy(
                kbuf.at[0], kbuf.at[i], ks_send.at[i], ks_recv.at[i], device_id=to, device_id_type=MESH
            ),
            pltpu.make_async_remote_copy(
                v_ref, vbuf.at[i], vs_send.at[i], vs_recv.at[i], device_id=to, device_id_type=MESH
            ),
        )

    def kv_start(i, c):
        a, b = kv_copies(i)
        a.start()
        b.start()
        return c

    lax.fori_loop(1, n_sp, kv_start, 0)

    q_rows = [[] for _ in range(heads_kv)]
    per_chunk = LANES // head
    for c in range(q_width // LANES):
        x = turn(q_ref[:, c * LANES : (c + 1) * LANES], q_gain) * head ** (-0.5)
        for part in range(per_chunk):
            kv = (c * per_chunk + part) // group
            want = kv % per_chunk
            y = x if part == want else pltpu.roll(x, head, 1)
            keep = low if want == 0 else jnp.logical_not(low)
            q_rows[kv].append(jnp.where(keep, y, 0.0).astype(bf16))

    n_slot = n_dev * pitch
    e_iota = lax.broadcasted_iota(jnp.int32, (n_dev, tok), 0)
    hit0 = (e_iota == ids_ref[0:1, :]).astype(f32)
    hit1 = (e_iota == ids_ref[1:2, :]).astype(f32)
    hits = hit0 + hit1
    before = (
        lax.broadcasted_iota(jnp.int32, (tok, tok), 0) < lax.broadcasted_iota(jnp.int32, (tok, tok), 1)
    ).astype(bf16)
    rank = dot(hits.astype(bf16), before)
    mark = (hits * (rank + 1.0)).astype(bf16)
    spread = (
        lax.broadcasted_iota(jnp.int32, (n_slot, n_dev), 0) // pitch
        == lax.broadcasted_iota(jnp.int32, (n_slot, n_dev), 1)
    ).astype(bf16)
    place = (lax.broadcasted_iota(jnp.int32, (n_slot, tok), 0) % pitch + 1).astype(f32)
    chosen = dot(spread, mark) == place
    pack[...] = chosen.astype(f32).astype(bf16)
    g = gate_ref[...]
    g_hi = g.astype(bf16).astype(f32)
    g_lo = g - g_hi
    for dst, part in ((comb_hi, g_hi), (comb_lo, g_lo)):
        both = (hit0 * part[0:1, :] + hit1 * part[1:2, :]).astype(bf16)
        dst[...] = jnp.where(chosen, dot(spread, both), 0.0).astype(bf16)

    def kv_wait(i, c):
        a, b = kv_copies(i)
        a.wait()
        b.wait()
        return c

    lax.fori_loop(1, n_sp, kv_wait, 0)

    keys = n_sp * tok
    outs = {}
    for kv in range(heads_kv):
        cols = slice(kv // per_chunk * LANES, (kv // per_chunk + 1) * LANES)
        k_all = kbuf[:, :, cols].reshape(keys, LANES)
        v_all = vbuf[:, :, cols].reshape(keys, LANES)
        for part in range(group):
            s = lax.dot_general(
                q_rows[kv][part], k_all, (((1,), (1,)), ((), ())), preferred_element_type=f32
            )
            p = jnp.exp(s - jnp.max(s, axis=-1, keepdims=True))
            total = jnp.sum(p, axis=-1, keepdims=True)
            outs[kv * group + part] = dot(p.astype(bf16), v_all) / total
    for c in range(q_width // LANES):
        piece = None
        for part in range(per_chunk):
            h = c * per_chunk + part
            have = (h // group) % per_chunk
            y = outs[h] if part == have else pltpu.roll(outs[h], head, 1)
            piece = y if piece is None else jnp.where(low, piece, y)
        att[:, c * LANES : (c + 1) * LANES] = piece.astype(bf16)

    weights[0].wait()
    projected = dot(att[...], wo[...])
    mixed = (res_ref[...].astype(f32) + rms(projected) * mix_ref[...]).astype(bf16)
    first[...] = mixed
    normed = (rms(mixed.astype(f32)) * ffn_ref[...]).astype(bf16)
    outbox[...] = dot(pack[...], normed).astype(bf16).reshape(n_dev, pitch, d_model)

    per_group = n_dev // groups
    order = [g_ for g_ in (2, 1, 3, 0) if g_ < groups]

    def dispatch(i):
        to = peer(i)
        return pltpu.make_async_remote_copy(
            outbox.at[to[0] * n_dp + to[1]], arrived.at[i], d_send.at[i], d_recv.at[i],
            device_id=to, device_id_type=MESH,
        )

    def answer(i):
        return pltpu.make_async_remote_copy(
            arrived.at[i], returned.at[sp * n_dp + dp], r_send.at[i], r_recv.at[i],
            device_id=source(i), device_id_type=MESH,
        )

    def start_d(i, c):
        dispatch(i).start()
        return c

    def wait_d(i, c):
        dispatch(i).wait()
        return c

    def start_r(i, c):
        answer(i).start()
        return c

    def wait_r(i, c):
        answer(i).wait()
        return c

    for gi in order:
        lax.fori_loop(max(gi * per_group, 1), (gi + 1) * per_group, start_d, 0)
    me = sp * n_dp + dp
    arrived[0] = outbox[me]
    for w in weights[1:]:
        w.wait()
    for gi in order:
        lo_, hi_ = gi * per_group, (gi + 1) * per_group
        lax.fori_loop(max(lo_, 1), hi_, wait_d, 0)
        x = arrived[lo_:hi_].reshape(per_group * pitch, d_model)
        gate_value = dot(x, wg[...])
        up_value = dot(x, wu[...])
        hidden = (gate_value / (1.0 + jnp.exp(-gate_value)) * up_value).astype(bf16)
        y = dot(hidden, wd[...]).astype(bf16)
        arrived[lo_:hi_] = y.reshape(per_group, pitch, d_model)
        lax.fori_loop(max(lo_, 1), hi_, start_r, 0)
    returned[me] = arrived[0]
    for gi in order:
        lax.fori_loop(max(gi * per_group, 1), (gi + 1) * per_group, wait_r, 0)

    back = returned[...].reshape(n_slot, d_model)
    dims = (((0,), (0,)), ((), ()))
    expert_sum = lax.dot_general(comb_hi[...], back, dims, preferred_element_type=f32)
    expert_sum += lax.dot_general(comb_lo[...], back, dims, preferred_element_type=f32)
    out_ref[...] = (first[...].astype(f32) + rms(expert_sum) * post_ref[...]).astype(bf16)


def shards(
    queries, keys, values, q_gain, k_gain, residual, out_weight, mix_gain, ffn_gain, post_gain,
    expert_ids, expert_gate, w_gate, w_up, w_down,
):
    n_sp = lax.axis_size("sp")
    n_dp = lax.axis_size("dp")
    n_dev = n_sp * n_dp
    tok = queries.shape[1]
    d_model = residual.shape[2]
    d_exp = w_gate.shape[2]
    head = q_gain.shape[0]
    kv_width = keys.shape[2]
    q_width = queries.shape[2]
    cap = 2 * tok * expert_ids.shape[2] // n_dev
    pitch = -(-cap // 16) * 16
    n_slot = n_dev * pitch
    vmem = pl.BlockSpec(memory_space=pltpu.VMEM)
    hbm = pl.BlockSpec(memory_space=pl.ANY)
    dma = pltpu.SemaphoreType.DMA
    result = pl.pallas_call(
        functools.partial(kernel, n_sp, n_dp, cap, pitch, 4),
        out_shape=jax.ShapeDtypeStruct((tok, d_model), bf16),
        in_specs=[vmem] * 15 + [hbm] * 4,
        out_specs=vmem,
        scratch_shapes=[
            pltpu.VMEM((n_sp, tok, kv_width), bf16),
            pltpu.VMEM((n_sp, tok, kv_width), bf16),
            pltpu.VMEM((tok, q_width), bf16),
            pltpu.VMEM((tok, d_model), bf16),
            pltpu.VMEM((n_dev, pitch, d_model), bf16),
            pltpu.VMEM((n_dev, pitch, d_model), bf16),
            pltpu.VMEM((n_dev, pitch, d_model), bf16),
            pltpu.VMEM((n_slot, tok), bf16),
            pltpu.VMEM((n_slot, tok), bf16),
            pltpu.VMEM((n_slot, tok), bf16),
            pltpu.VMEM((q_width, d_model), bf16),
            pltpu.VMEM((d_model, d_exp), bf16),
            pltpu.VMEM((d_model, d_exp), bf16),
            pltpu.VMEM((d_exp, d_model), bf16),
            dma((4,)),
            dma((n_sp,)), dma((n_sp,)), dma((n_sp,)), dma((n_sp,)),
            dma((n_dev,)), dma((n_dev,)), dma((n_dev,)), dma((n_dev,)),
        ],
        compiler_params=pltpu.CompilerParams(
            collective_id=0, has_side_effects=True, vmem_limit_bytes=63000000
        ),
    )(
        queries[0], keys[0], values[0], q_gain[None], k_gain[None],
        *tables(n_sp * tok // GRID, head),
        residual[0], mix_gain[None], ffn_gain[None], post_gain[None],
        expert_ids[0].T, expert_gate[0].T,
        out_weight, w_gate[0], w_up[0], w_down[0],
    )
    return result[None]


def solution(mesh):
    tokens = P("dp", "sp", None)
    experts = P(("sp", "dp"), None, None)
    return jax.shard_map(
        shards,
        mesh=mesh,
        in_specs=(tokens, tokens, tokens, P(), P(), tokens, P(), P(), P(), P(), tokens, tokens,
                  experts, experts, experts),
        out_specs=tokens,
        check_vma=False,
    )
```

time: 213 us -> 134 us (0.63)
  the two profiles are of different devices: /device:TPU:0 before, /device:TPU:9 now
where the time goes in v1:
time: 134 us; the launch traced here: 133 us
  Pallas kernels  131 us (98%)
  local copies, waits for them, and re-layouts  1.88 us (1%)
    pallas_call x1, Pallas kernels, shards(): pl.pallas_call(functools.partial(kernel, n_sp, n_dp, cap, pitch, 4), out_...  131 us

profile of v1, /device:TPU:9, one launch (start us, length us, event | category | flops | bytes accessed | tf_op | source)
XLA Modules:
  0.0 133.3 jit_solution(2948169119338292820)
XLA Ops:
  0.0 131.4 %shard_map.181 = bf16[128,2048]{1,0:T(8,128)(2,1)} custom-call(bf16[128,1024]{1,0:T(8,128)(2,1)} %bitcast.24, bf16[128,256]{1,0:T(8,128)(2,1)} %bitcast.25, bf16[128,256]{1,0:T(8,128)(2,1)} %bitcast.26, f32[1,64]{1,0:T(1,128)} %bitcast.32, f32[1,64]{1,0:T(1,128)} %bitcast.33, f32[16,128]{1,0:T(8,128)} %constant.8.clone.cr_ref, ...), custom_call_target="tpu_custom_call" | custom-call | tf_op jit(solution)/shard_map/pallas_call | solution.py:291
  131.5 1.9 %copy.21 = bf16[1,128,2048]{2,1,0:T(8,128)(2,1)} copy(bf16[1,128,2048]{2,1,0:T(8,128)(2,1)} %bitcast.19) | data formatting | bytes 1048576

commit v2 on v1

--- a/solution.py
+++ b/solution.py
@@ -45,16 +45,16 @@
 
 
 def kernel(
-    n_sp, n_dp, cap, pitch, groups,
+    n_sp, n_dp, pitch,
     q_ref, k_ref, v_ref, qg_ref, kg_ref, cr_ref, sr_ref, cc_ref, sc_ref,
     res_ref, mix_ref, ffn_ref, post_ref, ids_ref, gate_ref,
     wo_hbm, wg_hbm, wu_hbm, wd_hbm,
     out_ref,
     kbuf, vbuf, att, first, outbox, arrived, returned, pack, comb_hi, comb_lo,
+    ids_far, gate_far, rows_own, rows_far, part_own, part_far, x_send, x_recv,
     wo, wg, wu, wd, w_sem,
     ks_send, ks_recv, vs_send, vs_recv, d_send, d_recv, r_send, r_recv,
 ):
-    n_dev = n_sp * n_dp
     sp = lax.axis_index("sp")
     dp = lax.axis_index("dp")
     tok, q_width = q_ref.shape
@@ -71,11 +71,21 @@
     for w in weights:
         w.start()
 
+    span = n_sp // 2
+    n_half = span * n_dp
+    start = sp // span * span
+    place_sp = sp % span
+    partner = (lax.rem(sp + span, n_sp), dp)
+    base = start * n_dp
+
     def peer(i):
-        return lax.rem(sp + i // n_dp, n_sp), lax.rem(dp + i % n_dp, n_dp)
+        return start + lax.rem(place_sp + i // n_dp, span), lax.rem(dp + i % n_dp, n_dp)
 
     def source(i):
-        return lax.rem(sp + n_sp - i // n_dp, n_sp), lax.rem(dp + n_dp - i % n_dp, n_dp)
+        return (
+            start + lax.rem(place_sp + span - i // n_dp, span),
+            lax.rem(dp + n_dp - i % n_dp, n_dp),
+        )
 
     barrier = pltpu.get_barrier_semaphore()
 
@@ -83,7 +93,14 @@
         pl.semaphore_signal(barrier, inc=1, device_id=peer(i), device_id_type=MESH)
         return c
 
-    lax.fori_loop(1, n_dev, greet, 0)
+    def greet_far(i, c):
+        pl.semaphore_signal(
+            barrier, inc=1, device_id=(lax.rem(start + span + i, n_sp), dp), device_id_type=MESH
+        )
+        return c
+
+    lax.fori_loop(1, n_half, greet, 0)
+    lax.fori_loop(0, span, greet_far, 0)
 
     lane = lax.broadcasted_iota(jnp.int32, (tok, LANES), 1)
     even = lane % 2 == 0
@@ -117,7 +134,18 @@
         kbuf[0, :, cols] = turn(k_ref[:, cols], k_gain).astype(bf16)
     vbuf[0] = v_ref[...]
 
-    pl.semaphore_wait(barrier, n_dev - 1)
+    pl.semaphore_wait(barrier, n_half - 1 + span)
+
+    def exchange(n, src, dst):
+        return pltpu.make_async_remote_copy(
+            src, dst, x_send.at[n], x_recv.at[n], device_id=partner, device_id_type=MESH
+        )
+
+    tables_far = [exchange(0, ids_ref, ids_far), exchange(1, gate_ref, gate_far)]
+    rows_copy = exchange(2, rows_own, rows_far)
+    part_copy = exchange(3, part_own, part_far)
+    for copy in tables_far:
+        copy.start()
 
     def kv_copies(i):
         to = (lax.rem(sp + i, n_sp), dp)
@@ -149,29 +177,36 @@
             keep = low if want == 0 else jnp.logical_not(low)
             q_rows[kv].append(jnp.where(keep, y, 0.0).astype(bf16))
 
-    n_slot = n_dev * pitch
-    e_iota = lax.broadcasted_iota(jnp.int32, (n_dev, tok), 0)
-    hit0 = (e_iota == ids_ref[0:1, :]).astype(f32)
-    hit1 = (e_iota == ids_ref[1:2, :]).astype(f32)
-    hits = hit0 + hit1
+    n_slot = n_half * pitch
+    e_iota = lax.broadcasted_iota(jnp.int32, (n_half, tok), 0) + base
     before = (
         lax.broadcasted_iota(jnp.int32, (tok, tok), 0) < lax.broadcasted_iota(jnp.int32, (tok, tok), 1)
     ).astype(bf16)
-    rank = dot(hits.astype(bf16), before)
-    mark = (hits * (rank + 1.0)).astype(bf16)
     spread = (
-        lax.broadcasted_iota(jnp.int32, (n_slot, n_dev), 0) // pitch
-        == lax.broadcasted_iota(jnp.int32, (n_slot, n_dev), 1)
+        lax.broadcasted_iota(jnp.int32, (n_slot, n_half), 0) // pitch
+        == lax.broadcasted_iota(jnp.int32, (n_slot, n_half), 1)
     ).astype(bf16)
     place = (lax.broadcasted_iota(jnp.int32, (n_slot, tok), 0) % pitch + 1).astype(f32)
-    chosen = dot(spread, mark) == place
-    pack[...] = chosen.astype(f32).astype(bf16)
-    g = gate_ref[...]
-    g_hi = g.astype(bf16).astype(f32)
-    g_lo = g - g_hi
-    for dst, part in ((comb_hi, g_hi), (comb_lo, g_lo)):
-        both = (hit0 * part[0:1, :] + hit1 * part[1:2, :]).astype(bf16)
-        dst[...] = jnp.where(chosen, dot(spread, both), 0.0).astype(bf16)
+
+    def route(n, ids, gates):
+        hit0 = (e_iota == ids[0:1, :]).astype(f32)
+        hit1 = (e_iota == ids[1:2, :]).astype(f32)
+        hits = hit0 + hit1
+        rank = dot(hits.astype(bf16), before)
+        mark = (hits * (rank + 1.0)).astype(bf16)
+        chosen = dot(spread, mark) == place
+        pack[n] = chosen.astype(f32).astype(bf16)
+        g = gates[...]
+        g_hi = g.astype(bf16).astype(f32)
+        g_lo = g - g_hi
+        for dst, part in ((comb_hi, g_hi), (comb_lo, g_lo)):
+            both = (hit0 * part[0:1, :] + hit1 * part[1:2, :]).astype(bf16)
+            dst[n] = jnp.where(chosen, dot(spread, both), 0.0).astype(bf16)
+
+    route(0, ids_ref, gate_ref)
+    for copy in tables_far:
+        copy.wait()
+    route(1, ids_far, gate_far)
 
     def kv_wait(i, c):
         a, b = kv_copies(i)
@@ -207,65 +242,75 @@
     projected = dot(att[...], wo[...])
     mixed = (res_ref[...].astype(f32) + rms(projected) * mix_ref[...]).astype(bf16)
     first[...] = mixed
-    normed = (rms(mixed.astype(f32)) * ffn_ref[...]).astype(bf16)
-    outbox[...] = dot(pack[...], normed).astype(bf16).reshape(n_dev, pitch, d_model)
-
-    per_group = n_dev // groups
-    order = [g_ for g_ in (2, 1, 3, 0) if g_ < groups]
-
-    def dispatch(i):
+    rows_own[...] = (rms(mixed.astype(f32)) * ffn_ref[...]).astype(bf16)
+    rows_copy.start()
+
+    me = place_sp * n_dp + dp
+
+    def dispatch(n, i):
         to = peer(i)
         return pltpu.make_async_remote_copy(
-            outbox.at[to[0] * n_dp + to[1]], arrived.at[i], d_send.at[i], d_recv.at[i],
-            device_id=to, device_id_type=MESH,
-        )
-
-    def answer(i):
+            outbox.at[n, (to[0] - start) * n_dp + to[1]], arrived.at[n, i],
+            d_send.at[n, i], d_recv.at[n, i], device_id=to, device_id_type=MESH,
+        )
+
+    def answer(n, i):
         return pltpu.make_async_remote_copy(
-            arrived.at[i], returned.at[sp * n_dp + dp], r_send.at[i], r_recv.at[i],
+            arrived.at[n, i], returned.at[n, me], r_send.at[n, i], r_recv.at[n, i],
             device_id=source(i), device_id_type=MESH,
         )
 
-    def start_d(i, c):
-        dispatch(i).start()
-        return c
-
-    def wait_d(i, c):
-        dispatch(i).wait()
-        return c
-
-    def start_r(i, c):
-        answer(i).start()
-        return c
-
-    def wait_r(i, c):
-        answer(i).wait()
-        return c
-
-    for gi in order:
-        lax.fori_loop(max(gi * per_group, 1), (gi + 1) * per_group, start_d, 0)
-    me = sp * n_dp + dp
-    arrived[0] = outbox[me]
-    for w in weights[1:]:
-        w.wait()
-    for gi in order:
-        lo_, hi_ = gi * per_group, (gi + 1) * per_group
-        lax.fori_loop(max(lo_, 1), hi_, wait_d, 0)
-        x = arrived[lo_:hi_].reshape(per_group * pitch, d_model)
+    def each(make, act, n, lo_, hi_):
+        def step(i, c):
+            copy = make(n, i)
+            copy.start() if act == "start" else copy.wait()
+            return c
+
+        lax.fori_loop(max(lo_, 1), hi_, step, 0)
+
+    def send_rows(n, rows):
+        outbox[n] = dot(pack[n], rows).astype(bf16).reshape(n_half, pitch, d_model)
+        mid = n_half // 2
+        each(dispatch, "start", n, mid, n_half)
+        each(dispatch, "start", n, 0, mid)
+        arrived[n, 0] = outbox[n, me]
+
+    def experts(n, lo_, hi_):
+        x = arrived[n, lo_:hi_].reshape((hi_ - lo_) * pitch, d_model)
         gate_value = dot(x, wg[...])
         up_value = dot(x, wu[...])
         hidden = (gate_value / (1.0 + jnp.exp(-gate_value)) * up_value).astype(bf16)
         y = dot(hidden, wd[...]).astype(bf16)
-        arrived[lo_:hi_] = y.reshape(per_group, pitch, d_model)
-        lax.fori_loop(max(lo_, 1), hi_, start_r, 0)
-    returned[me] = arrived[0]
-    for gi in order:
-        lax.fori_loop(max(gi * per_group, 1), (gi + 1) * per_group, wait_r, 0)
-
-    back = returned[...].reshape(n_slot, d_model)
-    dims = (((0,), (0,)), ((), ()))
-    expert_sum = lax.dot_general(comb_hi[...], back, dims, preferred_element_type=f32)
-    expert_sum += lax.dot_general(comb_lo[...], back, dims, preferred_element_type=f32)
+        arrived[n, lo_:hi_] = y.reshape(hi_ - lo_, pitch, d_model)
+
+    def combine(n):
+        back = returned[n].reshape(n_slot, d_model)
+        dims = (((0,), (0,)), ((), ()))
+        total = lax.dot_general(comb_hi[n], back, dims, preferred_element_type=f32)
+        return total + lax.dot_general(comb_lo[n], back, dims, preferred_element_type=f32)
+
+    send_rows(0, rows_own[...])
+    for w in weights[1:]:
+        w.wait()
+    rows_copy.wait()
+    send_rows(1, rows_far[...])
+    each(dispatch, "wait", 0, 0, n_half)
+    experts(0, 0, n_half)
+    mid = n_half // 2
+    for lo_, hi_ in ((mid, n_half), (0, mid)):
+        each(dispatch, "wait", 1, lo_, hi_)
+        experts(1, lo_, hi_)
+        each(answer, "start", 1, lo_, hi_)
+    each(answer, "start", 0, 0, n_half)
+    for n in (0, 1):
+        returned[n, me] = arrived[n, 0]
+    each(answer, "wait", 1, 0, n_half)
+    part_own[...] = combine(1).astype(bf16)
+    part_copy.start()
+    each(answer, "wait", 0, 0, n_half)
+    near = combine(0)
+    part_copy.wait()
+    expert_sum = near + part_far[...].astype(f32)
     out_ref[...] = (first[...].astype(f32) + rms(expert_sum) * post_ref[...]).astype(bf16)
 
 
@@ -284,12 +329,14 @@
     q_width = queries.shape[2]
     cap = 2 * tok * expert_ids.shape[2] // n_dev
     pitch = -(-cap // 16) * 16
-    n_slot = n_dev * pitch
+    n_half = n_dev // 2
+    n_slot = n_half * pitch
+    top = expert_ids.shape[2]
     vmem = pl.BlockSpec(memory_space=pltpu.VMEM)
     hbm = pl.BlockSpec(memory_space=pl.ANY)
     dma = pltpu.SemaphoreType.DMA
     result = pl.pallas_call(
-        functools.partial(kernel, n_sp, n_dp, cap, pitch, 4),
+        functools.partial(kernel, n_sp, n_dp, pitch),
         out_shape=jax.ShapeDtypeStruct((tok, d_model), bf16),
         in_specs=[vmem] * 15 + [hbm] * 4,
         out_specs=vmem,
@@ -298,19 +345,26 @@
             pltpu.VMEM((n_sp, tok, kv_width), bf16),
             pltpu.VMEM((tok, q_width), bf16),
             pltpu.VMEM((tok, d_model), bf16),
-            pltpu.VMEM((n_dev, pitch, d_model), bf16),
-            pltpu.VMEM((n_dev, pitch, d_model), bf16),
-            pltpu.VMEM((n_dev, pitch, d_model), bf16),
-            pltpu.VMEM((n_slot, tok), bf16),
-            pltpu.VMEM((n_slot, tok), bf16),
-            pltpu.VMEM((n_slot, tok), bf16),
+            pltpu.VMEM((2, n_half, pitch, d_model), bf16),
+            pltpu.VMEM((2, n_half, pitch, d_model), bf16),
+            pltpu.VMEM((2, n_half, pitch, d_model), bf16),
+            pltpu.VMEM((2, n_slot, tok), bf16),
+            pltpu.VMEM((2, n_slot, tok), bf16),
+            pltpu.VMEM((2, n_slot, tok), bf16),
+            pltpu.VMEM((top, tok), jnp.int32),
+            pltpu.VMEM((top, tok), f32),
+            pltpu.VMEM((tok, d_model), bf16),
+            pltpu.VMEM((tok, d_model), bf16),
+            pltpu.VMEM((tok, d_model), bf16),
+            pltpu.VMEM((tok, d_model), bf16),
+            dma((4,)), dma((4,)),
             pltpu.VMEM((q_width, d_model), bf16),
             pltpu.VMEM((d_model, d_exp), bf16),
             pltpu.VMEM((d_model, d_exp), bf16),
             pltpu.VMEM((d_exp, d_model), bf16),
             dma((4,)),
             dma((n_sp,)), dma((n_sp,)), dma((n_sp,)), dma((n_sp,)),
-            dma((n_dev,)), dma((n_dev,)), dma((n_dev,)), dma((n_dev,)),
+            dma((2, n_half)), dma((2, n_half)), dma((2, n_half)), dma((2, n_half)),
         ],
         compiler_params=pltpu.CompilerParams(
             collective_id=0, has_side_effects=True, vmem_limit_bytes=63000000

time: 134 us -> 121 us (0.903)
  the two profiles are of different devices: /device:TPU:9 before, /device:TPU:0 now
where the time goes in v2:
time: 121 us
  Pallas kernels  119 us (98%)
  local copies, waits for them, and re-layouts  1.88 us (2%)
    pallas_call x1, Pallas kernels, shards(): pl.pallas_call(functools.partial(kernel, n_sp, n_dp, pitch), out_shape=ja...  119 us

profile of v2, /device:TPU:0, one launch (start us, length us, event | category | flops | bytes accessed | tf_op | source)
XLA Modules:
  0.0 120.8 jit_solution(15679879233315263967)
XLA Ops:
  0.0 118.9 %shard_map.181 = bf16[128,2048]{1,0:T(8,128)(2,1)} custom-call(bf16[128,1024]{1,0:T(8,128)(2,1)} %bitcast.24, bf16[128,256]{1,0:T(8,128)(2,1)} %bitcast.25, bf16[128,256]{1,0:T(8,128)(2,1)} %bitcast.26, f32[1,64]{1,0:T(1,128)} %bitcast.32, f32[1,64]{1,0:T(1,128)} %bitcast.33, f32[16,128]{1,0:T(8,128)} %constant.8.clone.cr_ref, ...), custom_call_target="tpu_custom_call" | custom-call | tf_op jit(solution)/shard_map/pallas_call | solution.py:338
  118.9 1.9 %copy.21 = bf16[1,128,2048]{2,1,0:T(8,128)(2,1)} copy(bf16[1,128,2048]{2,1,0:T(8,128)(2,1)} %bitcast.19) | data formatting | bytes 1048576
